TPU v7x, 32 devices: a whole 2x2x4 slice. The times are simulated.
32 devices in a mesh: sp: 8 (over z, x), tp: 4 (over y, core).
Axes of the slice: x: 2, y: 2, z: 4, core: 2. Of those that a mesh axis runs over, the one named last changes fastest.
Arguments:
- inputs: bfloat16 [8192, 2048], P('sp'), may hold values from -6 to 6
- w_query: bfloat16 [2048, 2048], P(None, 'tp'), may hold values from -0.125 to 0.125
- w_key: bfloat16 [2048, 2048], P(None, 'tp'), may hold values from -0.125 to 0.125
- w_value: bfloat16 [2048, 2048], P(None, 'tp'), may hold values from -0.125 to 0.125
- rel_table: float32 [16, 257], P('tp'), may hold values from -4 to 254
- out_grad: bfloat16 [8192, 2048], P('sp', 'tp'), may hold values from -6 to 6
Outputs:
- query_grad: bfloat16 [8192, 2048], P('sp', 'tp')
- key_grad: bfloat16 [8192, 2048], P('sp', 'tp')
- value_grad: bfloat16 [8192, 2048], P('sp', 'tp')
- query_weight_grad: float32 [2048, 2048], P('sp', 'tp')
- key_weight_grad: float32 [2048, 2048], P('sp', 'tp')
- value_weight_grad: float32 [2048, 2048], P('sp', 'tp')
- table_grad: float32 [16, 257], P('tp')
All inputs are finite; a program needn't handle non-finite values.
Results may differ from a plain program's by a relative error of at most 0.017.
The roundings to bfloat16 on the way count: a program that leaves them out, or rounds other values in their place, can miss the bound.
Values may be sent and summed in bfloat16 or wider, within the bound.
A program may use at most 128 MiB of HBM per device.

v0:
```python
import jax
import jax.numpy as jnp
from jax import lax
from jax.experimental import pallas as pl
from jax.experimental.pallas import tpu as pltpu
from jax.sharding import PartitionSpec as P


HDIM = 128
SEG = 64
PREV = 4
MAXREL = 128
REACH = PREV * SEG
TILE = 2 * SEG
BAND = REACH + TILE
WRAP = 4 * MAXREL
GROUPS = 2


def from_behind(block, axis, distance):
    devices = range(lax.axis_size(axis))
    route = [(i - distance, i) for i in devices if i - distance in devices]
    return lax.ppermute(block, axis, route)


def project(inputs, weight):
    return jnp.dot(inputs, weight, preferred_element_type=jnp.float32).astype(jnp.bfloat16)


def contract(a, b, dims):
    return lax.dot_general(a, b, (dims, ((), ())), preferred_element_type=jnp.float32)


def attention_kernel(
    first_ref, bias_ref, q_ref, k_ref, v_ref, g_ref, hk_ref, hv_ref,
    dq_ref, dk_ref, dv_ref, hdk_ref, hdv_ref, tk_ref, tv_ref, diag_ref,
    kx, vx, dk_acc, dv_acc, band_acc,
):
    rows = q_ref.shape[0]
    scale = HDIM ** (-0.5)
    kx[:REACH] = hk_ref[...]
    kx[REACH:] = k_ref[...]
    vx[:REACH] = hv_ref[...]
    vx[REACH:] = v_ref[...]
    dk_acc[...] = jnp.zeros_like(dk_acc)
    dv_acc[...] = jnp.zeros_like(dv_acc)
    band_acc[...] = jnp.zeros_like(band_acc)
    row = lax.broadcasted_iota(jnp.int32, (TILE, BAND), 0)
    col = lax.broadcasted_iota(jnp.int32, (TILE, BAND), 1)
    start = row // SEG * SEG
    seen = (col >= start) & (col < start + REACH + SEG)
    wide = jnp.broadcast_to(bias_ref[0], (TILE, WRAP))
    bias = pltpu.roll(wide, 0, 1, stride=1, stride_axis=0)[:, :BAND]
    bias = jnp.where(seen, bias, -jnp.inf)
    is_first = first_ref[0] == 0
    for blk in range(rows // TILE):
        lo = blk * TILE
        q = q_ref[lo : lo + TILE]
        g = g_ref[lo : lo + TILE]
        k = kx[lo : lo + BAND]
        v = vx[lo : lo + BAND]
        s = contract(q, k, ((1,), (1,))) * scale + bias
        if lo < REACH:
            s = jnp.where(is_first & (col < REACH - lo), -jnp.inf, s)
        m = jnp.max(s, axis=1, keepdims=True)
        e = jnp.exp(s - m)
        p = e * (1.0 / jnp.sum(e, axis=1, keepdims=True))
        p_low = p.astype(jnp.bfloat16)
        out = contract(p_low, v, ((1,), (0,))).astype(jnp.bfloat16)
        out_dot = jnp.sum(g.astype(jnp.float32) * out.astype(jnp.float32), axis=1, keepdims=True)
        dp = contract(g, v, ((1,), (1,)))
        ds = p * (dp - out_dot)
        ds_low = ds.astype(jnp.bfloat16)
        band_acc[:, :BAND] += ds
        dq_ref[lo : lo + TILE] = (contract(ds_low, k, ((1,), (0,))) * scale).astype(jnp.bfloat16)
        dk_acc[lo : lo + BAND] += contract(ds_low, q, ((0,), (0,)))
        dv_acc[lo : lo + BAND] += contract(p_low, g, ((0,), (0,)))
    dk_ref[...] = (dk_acc[REACH:] * scale).astype(jnp.bfloat16)
    dv_ref[...] = dv_acc[REACH:].astype(jnp.bfloat16)
    hdk_ref[...] = (dk_acc[:REACH] * scale).astype(jnp.bfloat16)
    hdv_ref[...] = dv_acc[:REACH].astype(jnp.bfloat16)
    tk_ref[...] = dk_acc[rows:] * scale
    tv_ref[...] = dv_acc[rows:]
    total = band_acc[...]
    half = TILE // 2
    while half >= 1:
        total = total[:half] + pltpu.roll(total[half:], WRAP - half, 1)
        half //= 2
    diag_ref[0] = total


def attention(first, bias_rows, query, keys, values, upstream, halo_k, halo_v, head0, heads):
    rows = query.shape[0]
    whole = pl.BlockSpec((rows, HDIM), lambda h: (0, h))
    shifted = pl.BlockSpec((rows, HDIM), lambda h: (0, head0 + h))
    edge = pl.BlockSpec((REACH, HDIM), lambda h: (0, h))
    line = pl.BlockSpec((1, 1, WRAP), lambda h: (head0 + h, 0, 0))
    width = heads * HDIM
    sds = jax.ShapeDtypeStruct
    flops = 12 * heads * rows * BAND * HDIM
    return pl.pallas_call(
        attention_kernel,
        grid=(heads,),
        in_specs=[pl.BlockSpec(memory_space=pltpu.SMEM), line, shifted, shifted, shifted, shifted,
                  pl.BlockSpec((REACH, HDIM), lambda h: (0, h)), pl.BlockSpec((REACH, HDIM), lambda h: (0, h))],
        out_specs=[whole, whole, whole, edge, edge, edge, edge,
                   pl.BlockSpec((1, 1, WRAP), lambda h: (h, 0, 0))],
        out_shape=[
            sds((rows, width), jnp.bfloat16), sds((rows, width), jnp.bfloat16), sds((rows, width), jnp.bfloat16),
            sds((REACH, width), jnp.bfloat16), sds((REACH, width), jnp.bfloat16),
            sds((REACH, width), jnp.float32), sds((REACH, width), jnp.float32),
            sds((heads, 1, WRAP), jnp.float32),
        ],
        scratch_shapes=[
            pltpu.VMEM((rows + REACH, HDIM), jnp.bfloat16), pltpu.VMEM((rows + REACH, HDIM), jnp.bfloat16),
            pltpu.VMEM((rows + REACH, HDIM), jnp.float32), pltpu.VMEM((rows + REACH, HDIM), jnp.float32),
            pltpu.VMEM((TILE, WRAP), jnp.float32),
        ],
        cost_estimate=pl.CostEstimate(flops=flops * 2, bytes_accessed=heads * rows * HDIM * 20, transcendentals=heads * rows * BAND),
    )(first, bias_rows, query, keys, values, upstream, halo_k, halo_v)


def swap(block, bit):
    size = lax.axis_size("sp")
    return lax.ppermute(block, "sp", [(i, i ^ (1 << bit)) for i in range(size)])


def side(pieces, lead, want):
    low = len(pieces)
    return [pieces[r] for r in range(low) if (r >> lead & 1) == want]


def product(lhs, grads):
    parts = [jnp.einsum("td,tc->dc", piece, grads, preferred_element_type=jnp.float32) for piece in lhs]
    return parts


def leading(pieces, grads, order):
    return jnp.concatenate([p.astype(jnp.bfloat16) for p in product(side(pieces, order[0], 1), grads)], axis=0)


def remainder(pieces, grads, order, came):
    total = jnp.concatenate(product(side(pieces, order[0], 0), grads), axis=0)
    return total + came.astype(jnp.float32)


def split(total, kept, bit):
    depth = total.shape[0] // len(kept)
    out = [i for i, r in enumerate(kept) if r >> bit & 1]
    stay = [i for i, r in enumerate(kept) if not r >> bit & 1]
    pick = lambda which: jnp.concatenate([total[i * depth : (i + 1) * depth] for i in which], axis=0)
    return pick(out).astype(jnp.bfloat16), pick(stay), [kept[i] for i in stay]


def local(inputs, w_query, w_key, w_value, rel_table, out_grad):
    rows, model = inputs.shape
    head_count = w_query.shape[1] // HDIM
    size = lax.axis_size("sp")
    bits = size.bit_length() - 1
    me = lax.axis_index("sp")
    first = me.reshape(1)
    far = rel_table[:, 2 * MAXREL :]
    pad = jnp.broadcast_to(far, (head_count, MAXREL))
    bias_rows = jnp.concatenate([pad, rel_table[:, :0:-1], pad], axis=1)[:, None, :]
    keys = project(inputs, w_key)
    values = project(inputs, w_value)
    halo = from_behind(jnp.concatenate([keys[rows - REACH :], values[rows - REACH :]], axis=1), "sp", 1)
    query = project(inputs, w_query)
    width = head_count * HDIM
    heads = head_count // GROUPS
    span = heads * HDIM
    depth = model // size
    block = lambda r: lax.dynamic_slice(inputs, (0, (me ^ r) * depth), (rows, depth))
    low = min(size, 4)
    members = [[r for r in range(size) if r % low == p] for p in range(low)]
    pieces = [jnp.concatenate([block(r) for r in rs], axis=1) for rs in members]
    orders, ready = chunk_plan(bits)
    grads, chunks, flying, diags = [], [], [], []
    for group in range(GROUPS):
        at = group * span
        dq, dk, dv, hdk, hdv, tk, tv, diag = attention(
            first, bias_rows, query, keys, values, out_grad,
            halo[:, at : at + span], halo[:, width + at : width + at + span], group * heads, heads)
        back = jnp.concatenate([hdk, hdv], axis=1)
        sent = leading(pieces, dq, orders[3 * group])
        if group + 1 < GROUPS:
            back, sent, query = lax.optimization_barrier((back, sent, query))
        back = from_behind(back, "sp", -1).astype(jnp.float32)
        flying.append(swap(sent, orders[3 * group][0]))
        dk = lax.dynamic_update_slice(dk, (tk + back[:, :span]).astype(jnp.bfloat16), (rows - REACH, 0))
        dv = lax.dynamic_update_slice(dv, (tv + back[:, span:]).astype(jnp.bfloat16), (rows - REACH, 0))
        for i, grad in ((1, dk), (2, dv)):
            order = orders[3 * group + i]
            flying.append(swap(leading(pieces, grad, order), order[0]))
        grads.append((dq, dk, dv))
        chunks.extend((dq, dk, dv))
        diags.append(diag)
    count = len(chunks)
    kept = [[r for p in range(low) if not p >> order[0] & 1 for r in members[p]] for order in orders]
    held = [None] * count
    steps = sorted(((c, s) for c in range(count) for s in range(bits)), key=lambda cs: (ready[cs[0]] + 0.95 * cs[1], cs))
    last = None
    for c, stage in steps:
        came = flying[c]
        if last is not None:
            came, held[last] = lax.optimization_barrier((came, held[last]))
        if stage == 0:
            held[c] = remainder(pieces, chunks[c], orders[c], came)
        else:
            held[c] = held[c] + came.astype(jnp.float32)
        if stage + 1 < bits:
            bit = orders[c][stage + 1]
            out, held[c], kept[c] = split(held[c], kept[c], bit)
            flying[c] = swap(out, bit)
        last = c
    sums = [held[3 * group : 3 * group + 3] for group in range(GROUPS)]
    query_grad, key_grad, value_grad = [jnp.concatenate(parts, axis=1) for parts in zip(*grads)]
    wq, wk, wv = [jnp.concatenate(parts, axis=1) for parts in zip(*sums)]
    diag = jnp.concatenate(diags, axis=0)[:, 0, :]
    diag, _ = lax.optimization_barrier((diag, held[0]))
    for bit in range(bits):
        diag = diag + swap(diag, bit)
    top = jnp.sum(diag[:, : MAXREL + 1], axis=1, keepdims=True) + jnp.sum(diag[:, 3 * MAXREL :], axis=1, keepdims=True)
    table_grad = jnp.concatenate(
        [jnp.zeros((head_count, 1), jnp.float32), diag[:, MAXREL + 1 : 3 * MAXREL][:, ::-1], top], axis=1)
    return query_grad, key_grad, value_grad, wq, wk, wv, table_grad


def chunk_plan(bits):
    plain = list(range(bits))
    turned = [1, 0] + plain[2:] if bits > 1 else plain
    count = 3 * GROUPS
    orders = [plain] * (count - 2) + [turned] * 2
    ready = [1.0 + i for i in range(count - 2)] + [count - 2.1, count - 1.9]
    return orders, ready


def solution(mesh):
    placed = (
        P("sp", None),
        P(None, "tp"),
        P(None, "tp"),
        P(None, "tp"),
        P("tp", None),
        P("sp", "tp"),
    )
    return jax.shard_map(
        local,
        mesh=mesh,
        in_specs=placed,
        out_specs=(
            P("sp", "tp"),
            P("sp", "tp"),
            P("sp", "tp"),
            P("sp", "tp"),
            P("sp", "tp"),
            P("sp", "tp"),
            P("tp", None),
        ),
        check_vma=False,
    )
```

profile of v0, /device:TPU:0, one launch (start us, length us, event | category | flops | bytes accessed | tf_op | source)
XLA Modules:
  0.0 193.9 jit_solution(17746297546967190666)
XLA Ops:
  0.7 1.6 copy-done
  2.2 5.2 %convolution_convert_fusion.1.k_ref = bf16[1024,512]{1,0:T(8,128)(2,1)S(1)} fusion(bf16[1024,2048]{1,0:T(8,128)(2,1)} %param.6, bf16[2048,512]{1,0:T(8,128)(2,1)S(1)} %copy-done), kind=kOutput, calls=%fused_computation.1 | convolution fusion | flops 2148007936 | bytes 7340032 | tf_op jit(solution)/shard_map/dot_general | solution.py:27
  7.5 2.3 %convolution_convert_fusion.v_ref = bf16[1024,512]{1,0:T(8,128)(2,1)S(1)} fusion(bf16[1024,2048]{1,0:T(8,128)(2,1)S(1)} %copy-done.2, bf16[2048,512]{1,0:T(8,128)(2,1)S(1)} %copy-done.42), kind=kOutput, calls=%fused_computation | convolution fusion | flops 2148007936 | bytes 7340032 | tf_op jit(solution)/shard_map/dot_general | solution.py:27
  10.9 5.1 %collective-permute-start = (bf16[256,1024]{1,0:T(8,128)(2,1)S(1)}, bf16[256,1024]{1,0:T(8,128)(2,1)S(1)}, u32[]{:S(2)}, u32[]{:S(2)}) collective-permute-start(bf16[256,1024]{1,0:T(8,128)(2,1)S(1)} %pad_maximum_fusion.7), channel_id=1, source_target_pairs={{0,4},{4,8},{8,12},{12,16},{16,20},{20,24},{24,28},{1,5},{5,9},{9,... | collective-permute-start | bytes 1572872 | tf_op jit(solution)/shard_map/ppermute | solution.py:23
  17.1 3.8 %constant_dynamic-slice_fusion.1 = (bf16[1024,256]{1,0:T(8,128)(2,1)}, bf16[1024,256]{1,0:T(8,128)(2,1)S(1)}, bf16[1024,256]{1,0:T(8,128)(2,1)S(1)}, bf16[1024,2...) fusion(bf16[1024,2048]{1,0:T(8,128)(2,1)} %param.6, ...), kind=kLoop, calls=%fused_computation.82 | loop fusion | bytes 8388640 | tf_op jit(solution)/shard_map/dynamic_slice | solution.py:173
  22.1 3.3 %convolution_convert_fusion.2.q_ref = bf16[1024,512]{1,0:T(8,128)(2,1)} fusion(bf16[1024,2048]{1,0:T(8,128)(2,1)S(1)} %copy-done.3, bf16[2048,512]{1,0:T(8,128)(2,1)S(1)} %copy-done.43), kind=kOutput, calls=%fused_computation.2 | convolution fusion | flops 2148007936 | bytes 7340032 | tf_op jit(solution)/shard_map/dot_general | solution.py:27
  25.4 1.6 collective-permute-done
  27.8 13.5 %shard_map.117 = (bf16[1024,256]{1,0:T(8,128)(2,1)}, bf16[1024,256]{1,0:T(8,128)(2,1)}, bf16[1024,256]{1,0:T(8,128)(2,1)}, bf16[256,256]{1,0:T(8,128)(2,1)}, bf1...) custom-call(s32[1]{0:T(128)} %bitcast.first_ref, ...), custom_call_target="tpu_custom_call" | custom-call | flops 2415919104 | bytes 5242880 | tf_op jit(solution)/shard_map/pallas_call | solution.py:101
  41.3 1.6 convolution_convert_fusion.14
  44.0 13.6 %shard_map.118 = (bf16[1024,256]{1,0:T(8,128)(2,1)}, bf16[1024,256]{1,0:T(8,128)(2,1)}, bf16[1024,256]{1,0:T(8,128)(2,1)}, bf16[256,256]{1,0:T(8,128)(2,1)}, bf1...) custom-call(s32[1]{0:T(128)} %bitcast.first_ref, ...), custom_call_target="tpu_custom_call" | custom-call | flops 2415919104 | bytes 5242880 | tf_op jit(solution)/shard_map/pallas_call | solution.py:101
  57.5 1.9 convolution_convert_fusion.3
  60.5 1.6 fusion.12
  63.1 1.5 collective-permute-start.1
  64.6 3.2 %collective-permute-start.4 = (bf16[1024,256]{1,0:T(8,128)(2,1)S(1)}, bf16[1024,256]{1,0:T(8,128)(2,1)S(1)}, u32[]{:S(2)}, u32[]{:S(2)}) collective-permute-start(bf16[1024,256]{1,0:T(8,128)(2,1)S(1)} %pad_maximum_fusion.8), channel_id=1, source_target_pairs={{0,4},{4,0},{8,12},{12,8},{16,20},{20,16},{24,28},{28,24},{1,5},{5... | collective-permute-start | bytes 1572872 | tf_op jit(solution)/shard_map/ppermute | solution.py:125
  67.9 1.3 collective-permute-start.2
  70.0 2.6 %collective-permute-start.13 = (bf16[1024,256]{1,0:T(8,128)(2,1)}, bf16[1024,256]{1,0:T(8,128)(2,1)}, u32[]{:S(2)}, u32[]{:S(2)}) collective-permute-start(bf16[1024,256]{1,0:T(8,128)(2,1)} %pad_maximum_fusion.13), channel_id=1, source_target_pairs={{0,4},{4,0},{8,12},{12,8},{16,20},{20,16},{24,28},{28,24},{1,5},{5... | collective-permute-start | bytes 1572872 | tf_op jit(solution)/shard_map/ppermute | solution.py:125
  73.2 1.3 fusion.8
  80.0 11.5 %collective-permute-done.2 = bf16[256,512]{1,0:T(8,128)(2,1)S(1)} collective-permute-done((bf16[256,512]{1,0:T(8,128)(2,1)S(1)}, bf16[256,512]{1,0:T(8,128)(2,1)S(1)}, u32[]{:S(2)}, u32[]{:S(2)}) %collective-permute-start.2) | collective-permute-done | bytes 262176 | tf_op jit(solution)/shard_map/ppermute | solution.py:23
  92.6 1.3 fusion.15
  94.9 1.5 pad_maximum_fusion.3
  96.5 1.3 fusion.19
  97.8 1.3 fusion.13
  99.2 3.1 %collective-permute-start.5 = (bf16[512,256]{1,0:T(8,128)(2,1)S(1)}, bf16[512,256]{1,0:T(8,128)(2,1)S(1)}, u32[]{:S(2)}, u32[]{:S(2)}) collective-permute-start(bf16[512,256]{1,0:T(8,128)(2,1)S(1)} %concatenate.183), channel_id=1, source_target_pairs={{0,8},{4,12},{8,0},{12,4},{16,24},{20,28},{24,16},{28,20},{1,9},{5... | collective-permute-start | bytes 786440 | tf_op jit(solution)/shard_map/ppermute | solution.py:125
  102.3 2.1 %collective-permute-start.9 = (bf16[1024,256]{1,0:T(8,128)(2,1)S(1)}, bf16[1024,256]{1,0:T(8,128)(2,1)S(1)}, u32[]{:S(2)}, u32[]{:S(2)}) collective-permute-start(bf16[1024,256]{1,0:T(8,128)(2,1)S(1)} %pad_maximum_fusion.11), channel_id=1, source_target_pairs={{0,4},{4,0},{8,12},{12,8},{16,20},{20,16},{24,28},{28,24},{1,5},{5... | collective-permute-start | bytes 1572872 | tf_op jit(solution)/shard_map/ppermute | solution.py:125
  104.4 1.3 fusion.18
  106.8 7.2 %collective-permute-done.3 = bf16[1024,256]{1,0:T(8,128)(2,1)S(1)} collective-permute-done((bf16[1024,256]{1,0:T(8,128)(2,1)S(1)}, bf16[1024,256]{1,0:T(8,128)(2,1)S(1)}, u32[]{:S(2)}, u32[]{:S(2)}) %collective-permute-start.3) | collective-permute-done | bytes 524320 | tf_op jit(solution)/shard_map/ppermute | solution.py:125
  114.0 4.0 %collective-permute-start.7 = (bf16[256,256]{1,0:T(8,128)(2,1)S(1)}, bf16[256,256]{1,0:T(8,128)(2,1)S(1)}, u32[]{:S(2)}, u32[]{:S(2)}) collective-permute-start(bf16[256,256]{1,0:T(8,128)(2,1)S(1)} %slice.216), channel_id=1, source_target_pairs={{0,16},{4,20},{8,24},{12,28},{16,0},{20,4},{24,8},{28,12},{1,17},{... | collective-permute-start | bytes 393224 | tf_op jit(solution)/shard_map/ppermute | solution.py:125
  118.1 1.6 collective-permute-start.6
  121.9 5.6 %collective-permute-done.6 = bf16[512,256]{1,0:T(8,128)(2,1)S(1)} collective-permute-done((bf16[512,256]{1,0:T(8,128)(2,1)S(1)}, bf16[512,256]{1,0:T(8,128)(2,1)S(1)}, u32[]{:S(2)}, u32[]{:S(2)}) %collective-permute-start.6) | collective-permute-done | bytes 262176 | tf_op jit(solution)/shard_map/ppermute | solution.py:125
  129.4 1.4 collective-permute-start.12
  131.1 2.5 %collective-permute-start.22 = (f32[4,512]{1,0:T(4,128)S(1)}, f32[4,512]{1,0:T(4,128)S(1)}, u32[]{:S(2)}, u32[]{:S(2)}) collective-permute-start(f32[4,512]{1,0:T(4,128)S(1)} %add.143), channel_id=1, source_target_pairs={{0,8},{4,12},{8,0},{12,4},{16,24},{20,28},{24,16},{28,20},{1,9},{5... | collective-permute-start | bytes 24584 | tf_op jit(solution)/shard_map/ppermute | solution.py:125
  133.7 13.7 %collective-permute-done.22 = f32[4,512]{1,0:T(4,128)S(1)} collective-permute-done((f32[4,512]{1,0:T(4,128)S(1)}, f32[4,512]{1,0:T(4,128)S(1)}, u32[]{:S(2)}, u32[]{:S(2)}) %collective-permute-start.22) | collective-permute-done | bytes 8224 | tf_op jit(solution)/shard_map/ppermute | solution.py:125
  147.4 1.3 collective-permute-start.23
  148.9 1.7 collective-permute-start.10
  150.6 1.4 collective-permute-done.23
  152.1 1.4 collective-permute-start.14
  154.8 1.6 collective-permute-done.10
  156.4 1.5 maximum_add_fusion.2
  158.0 3.0 %collective-permute-start.11 = (bf16[512,256]{1,0:T(8,128)(2,1)S(1)}, bf16[512,256]{1,0:T(8,128)(2,1)S(1)}, u32[]{:S(2)}, u32[]{:S(2)}) collective-permute-start(bf16[512,256]{1,0:T(8,128)(2,1)S(1)} %concatenate.181), channel_id=1, source_target_pairs={{0,4},{4,0},{8,12},{12,8},{16,20},{20,16},{24,28},{28,24},{1,5},{5... | collective-permute-start | bytes 786440 | tf_op jit(solution)/shard_map/ppermute | solution.py:125
  161.1 1.3 maximum_add_fusion.5
  162.6 1.5 maximum_add_fusion.4
  165.3 2.0 %collective-permute-start.16 = (bf16[512,256]{1,0:T(8,128)(2,1)S(1)}, bf16[512,256]{1,0:T(8,128)(2,1)S(1)}, u32[]{:S(2)}, u32[]{:S(2)}) collective-permute-start(bf16[512,256]{1,0:T(8,128)(2,1)S(1)} %concatenate.178), channel_id=1, source_target_pairs={{0,8},{4,12},{8,0},{12,4},{16,24},{20,28},{24,16},{28,20},{1,9},{5... | collective-permute-start | bytes 786440 | tf_op jit(solution)/shard_map/ppermute | solution.py:125
  167.3 1.2 collective-permute-start.15
  169.7 3.0 %collective-permute-done.17 = bf16[256,256]{1,0:T(8,128)(2,1)S(1)} collective-permute-done((bf16[256,256]{1,0:T(8,128)(2,1)S(1)}, bf16[256,256]{1,0:T(8,128)(2,1)S(1)}, u32[]{:S(2)}, u32[]{:S(2)}) %collective-permute-start.17) | collective-permute-done | bytes 131104 | tf_op jit(solution)/shard_map/ppermute | solution.py:125
  172.8 5.3 %collective-permute-done.16 = bf16[512,256]{1,0:T(8,128)(2,1)S(1)} collective-permute-done((bf16[512,256]{1,0:T(8,128)(2,1)S(1)}, bf16[512,256]{1,0:T(8,128)(2,1)S(1)}, u32[]{:S(2)}, u32[]{:S(2)}) %collective-permute-start.16) | collective-permute-done | bytes 262176 | tf_op jit(solution)/shard_map/ppermute | solution.py:125
  179.3 2.9 %collective-permute-start.18 = (bf16[256,256]{1,0:T(8,128)(2,1)S(1)}, bf16[256,256]{1,0:T(8,128)(2,1)S(1)}, u32[]{:S(2)}, u32[]{:S(2)}) collective-permute-start(bf16[256,256]{1,0:T(8,128)(2,1)S(1)} %slice.213), channel_id=1, source_target_pairs={{0,16},{4,20},{8,24},{12,28},{16,0},{20,4},{24,8},{28,12},{1,17},{... | collective-permute-start | bytes 393224 | tf_op jit(solution)/shard_map/ppermute | solution.py:125
  182.3 7.6 %collective-permute-done.19 = bf16[256,256]{1,0:T(8,128)(2,1)S(1)} collective-permute-done((bf16[256,256]{1,0:T(8,128)(2,1)S(1)}, bf16[256,256]{1,0:T(8,128)(2,1)S(1)}, u32[]{:S(2)}, u32[]{:S(2)}) %collective-permute-start.19) | collective-permute-done | bytes 131104 | tf_op jit(solution)/shard_map/ppermute | solution.py:125
  189.9 2.0 %collective-permute-done.18 = bf16[256,256]{1,0:T(8,128)(2,1)S(1)} collective-permute-done((bf16[256,256]{1,0:T(8,128)(2,1)S(1)}, bf16[256,256]{1,0:T(8,128)(2,1)S(1)}, u32[]{:S(2)}, u32[]{:S(2)}) %collective-permute-start.18) | collective-permute-done | bytes 131104 | tf_op jit(solution)/shard_map/ppermute | solution.py:125
  (204 shorter events, 29.2 us)
Async XLA Ops:
  0.6 6.8 %copy-start.2 = (bf16[1024,2048]{1,0:T(8,128)(2,1)S(1)}, bf16[1024,2048]{1,0:T(8,128)(2,1)}, u32[]{:S(2)}) copy-start(bf16[1024,2048]{1,0:T(8,128)(2,1)} %param.6) | copy-start | bytes 12582916
  0.7 6.8 %copy-start.42 = (bf16[2048,512]{1,0:T(8,128)(2,1)S(1)}, bf16[2048,512]{1,0:T(8,128)(2,1)}, u32[]{:S(2)}) copy-start(bf16[2048,512]{1,0:T(8,128)(2,1)} %param.9) | copy-start | bytes 6291460
  7.5 8.5 %copy-start.39 = (f32[4,257]{1,0:T(4,128)S(1)}, f32[4,257]{1,0:T(4,128)}, u32[]{:S(2)}) copy-start(f32[4,257]{1,0:T(4,128)} %param.10) | copy-start | bytes 12340
  10.9 16.1 %collective-permute-start = (bf16[256,1024]{1,0:T(8,128)(2,1)S(1)}, bf16[256,1024]{1,0:T(8,128)(2,1)S(1)}, u32[]{:S(2)}, u32[]{:S(2)}) collective-permute-start(bf16[256,1024]{1,0:T(8,128)(2,1)S(1)} %pad_maximum_fusion.7), channel_id=1, source_target_pairs={{0,4},{4,8},{8,12},{12,16},{16,20},{20,24},{24,28},{1,5},{5,9},{9,... | collective-permute-start | bytes 1572872 | tf_op jit(solution)/shard_map/ppermute | solution.py:23
  17.1 3.9 %copy-start.3 = (bf16[1024,2048]{1,0:T(8,128)(2,1)S(1)}, bf16[1024,2048]{1,0:T(8,128)(2,1)}, u32[]{:S(2)}) copy-start(bf16[1024,2048]{1,0:T(8,128)(2,1)} %param.6) | copy-start | bytes 12582916
  17.1 4.9 %copy-start.43 = (bf16[2048,512]{1,0:T(8,128)(2,1)S(1)}, bf16[2048,512]{1,0:T(8,128)(2,1)}, u32[]{:S(2)}) copy-start(bf16[2048,512]{1,0:T(8,128)(2,1)} %param.7) | copy-start | bytes 6291460
  22.1 37.4 %copy-start.17 = (bf16[1024,256]{1,0:T(8,128)(2,1)}, bf16[1024,256]{1,0:T(8,128)(2,1)S(1)}, u32[]{:S(2)}) copy-start(bf16[1024,256]{1,0:T(8,128)(2,1)S(1)} %get-tuple-element.121) | copy-start | bytes 1572868
  22.1 37.9 %copy-start.21 = (bf16[1024,256]{1,0:T(8,128)(2,1)}, bf16[1024,256]{1,0:T(8,128)(2,1)S(1)}, u32[]{:S(2)}) copy-start(bf16[1024,256]{1,0:T(8,128)(2,1)S(1)} %get-tuple-element.117) | copy-start | bytes 1572868
  22.1 38.4 %copy-start.19 = (bf16[1024,256]{1,0:T(8,128)(2,1)}, bf16[1024,256]{1,0:T(8,128)(2,1)S(1)}, u32[]{:S(2)}) copy-start(bf16[1024,256]{1,0:T(8,128)(2,1)S(1)} %get-tuple-element.116) | copy-start | bytes 1572868
  60.5 7.3 %copy-start.33 = (bf16[256,256]{1,0:T(8,128)(2,1)S(1)}, bf16[256,256]{1,0:T(8,128)(2,1)}, u32[]{:S(2)}) copy-start(bf16[256,256]{1,0:T(8,128)(2,1)} %get-tuple-element.71) | copy-start | bytes 393220
  60.5 7.3 %copy-start.34 = (bf16[256,256]{1,0:T(8,128)(2,1)S(1)}, bf16[256,256]{1,0:T(8,128)(2,1)}, u32[]{:S(2)}) copy-start(bf16[256,256]{1,0:T(8,128)(2,1)} %get-tuple-element.72) | copy-start | bytes 393220
  62.0 10.6 %copy-start.23 = (bf16[1024,256]{1,0:T(8,128)(2,1)S(1)}, bf16[1024,256]{1,0:T(8,128)(2,1)}, u32[]{:S(2)}) copy-start(bf16[1024,256]{1,0:T(8,128)(2,1)} %get-tuple-element.115) | copy-start | bytes 1572868
  62.1 10.6 %copy-start.24 = (bf16[1024,256]{1,0:T(8,128)(2,1)S(1)}, bf16[1024,256]{1,0:T(8,128)(2,1)}, u32[]{:S(2)}) copy-start(bf16[1024,256]{1,0:T(8,128)(2,1)} %get-tuple-element.122) | copy-start | bytes 1572868
  63.1 11.5 %collective-permute-start.1 = (bf16[256,512]{1,0:T(8,128)(2,1)S(1)}, bf16[256,512]{1,0:T(8,128)(2,1)S(1)}, u32[]{:S(2)}, u32[]{:S(2)}) collective-permute-start(bf16[256,512]{1,0:T(8,128)(2,1)S(1)} %pad_maximum_fusion.17), channel_id=1, source_target_pairs={{4,0},{8,4},{12,8},{16,12},{20,16},{24,20},{28,24},{5,1},{9,5},{13... | collective-permute-start | bytes 786440 | tf_op jit(solution)/shard_map/ppermute | solution.py:23
  64.6 34.4 %collective-permute-start.4 = (bf16[1024,256]{1,0:T(8,128)(2,1)S(1)}, bf16[1024,256]{1,0:T(8,128)(2,1)S(1)}, u32[]{:S(2)}, u32[]{:S(2)}) collective-permute-start(bf16[1024,256]{1,0:T(8,128)(2,1)S(1)} %pad_maximum_fusion.8), channel_id=1, source_target_pairs={{0,4},{4,0},{8,12},{12,8},{16,20},{20,16},{24,28},{28,24},{1,5},{5... | collective-permute-start | bytes 1572872 | tf_op jit(solution)/shard_map/ppermute | solution.py:125
  67.8 5.3 %copy-start.40 = (f32[2,1,512]{2,1,0:T(1,128)S(1)}, f32[2,1,512]{2,1,0:T(1,128)}, u32[]{:S(2)}) copy-start(f32[2,1,512]{2,1,0:T(1,128)} %get-tuple-element.112) | copy-start | bytes 12292
  67.8 5.3 %copy-start.41 = (f32[2,1,512]{2,1,0:T(1,128)S(1)}, f32[2,1,512]{2,1,0:T(1,128)}, u32[]{:S(2)}) copy-start(f32[2,1,512]{2,1,0:T(1,128)} %get-tuple-element.113) | copy-start | bytes 12292
  67.9 23.6 %collective-permute-start.2 = (bf16[256,512]{1,0:T(8,128)(2,1)S(1)}, bf16[256,512]{1,0:T(8,128)(2,1)S(1)}, u32[]{:S(2)}, u32[]{:S(2)}) collective-permute-start(bf16[256,512]{1,0:T(8,128)(2,1)S(1)} %pad_maximum_fusion.18), channel_id=1, source_target_pairs={{4,0},{8,4},{12,8},{16,12},{20,16},{24,20},{28,24},{5,1},{9,5},{13... | collective-permute-start | bytes 786440 | tf_op jit(solution)/shard_map/ppermute | solution.py:23
  70.0 91.1 %collective-permute-start.13 = (bf16[1024,256]{1,0:T(8,128)(2,1)}, bf16[1024,256]{1,0:T(8,128)(2,1)}, u32[]{:S(2)}, u32[]{:S(2)}) collective-permute-start(bf16[1024,256]{1,0:T(8,128)(2,1)} %pad_maximum_fusion.13), channel_id=1, source_target_pairs={{0,4},{4,0},{8,12},{12,8},{16,20},{20,16},{24,28},{28,24},{1,5},{5... | collective-permute-start | bytes 1572872 | tf_op jit(solution)/shard_map/ppermute | solution.py:125
  79.5 12.1 %copy-start.13 = (bf16[1024,256]{1,0:T(8,128)(2,1)S(1)}, bf16[1024,256]{1,0:T(8,128)(2,1)}, u32[]{:S(2)}) copy-start(bf16[1024,256]{1,0:T(8,128)(2,1)} %get-tuple-element.69) | copy-start | bytes 1572868
  79.5 12.1 %copy-start.14 = (bf16[1024,256]{1,0:T(8,128)(2,1)S(1)}, bf16[1024,256]{1,0:T(8,128)(2,1)}, u32[]{:S(2)}) copy-start(bf16[1024,256]{1,0:T(8,128)(2,1)} %get-tuple-element.75) | copy-start | bytes 1572868
  79.5 12.1 %copy-start.29 = (f32[256,256]{1,0:T(8,128)S(1)}, f32[256,256]{1,0:T(8,128)}, u32[]{:S(2)}) copy-start(f32[256,256]{1,0:T(8,128)} %get-tuple-element.70) | copy-start | bytes 786436
  79.5 12.1 %copy-start.30 = (f32[256,256]{1,0:T(8,128)S(1)}, f32[256,256]{1,0:T(8,128)}, u32[]{:S(2)}) copy-start(f32[256,256]{1,0:T(8,128)} %get-tuple-element.76) | copy-start | bytes 786436
  96.4 17.5 %collective-permute-start.3 = (bf16[1024,256]{1,0:T(8,128)(2,1)S(1)}, bf16[1024,256]{1,0:T(8,128)(2,1)S(1)}, u32[]{:S(2)}, u32[]{:S(2)}) collective-permute-start(bf16[1024,256]{1,0:T(8,128)(2,1)S(1)} %pad_maximum_fusion.9), channel_id=1, source_target_pairs={{0,4},{4,0},{8,12},{12,8},{16,20},{20,16},{24,28},{28,24},{1,5},{5... | collective-permute-start | bytes 1572872 | tf_op jit(solution)/shard_map/ppermute | solution.py:125
  99.2 7.4 %collective-permute-start.5 = (bf16[512,256]{1,0:T(8,128)(2,1)S(1)}, bf16[512,256]{1,0:T(8,128)(2,1)S(1)}, u32[]{:S(2)}, u32[]{:S(2)}) collective-permute-start(bf16[512,256]{1,0:T(8,128)(2,1)S(1)} %concatenate.183), channel_id=1, source_target_pairs={{0,8},{4,12},{8,0},{12,4},{16,24},{20,28},{24,16},{28,20},{1,9},{5... | collective-permute-start | bytes 786440 | tf_op jit(solution)/shard_map/ppermute | solution.py:125
  102.3 31.4 %collective-permute-start.9 = (bf16[1024,256]{1,0:T(8,128)(2,1)S(1)}, bf16[1024,256]{1,0:T(8,128)(2,1)S(1)}, u32[]{:S(2)}, u32[]{:S(2)}) collective-permute-start(bf16[1024,256]{1,0:T(8,128)(2,1)S(1)} %pad_maximum_fusion.11), channel_id=1, source_target_pairs={{0,4},{4,0},{8,12},{12,8},{16,20},{20,16},{24,28},{28,24},{1,5},{5... | collective-permute-start | bytes 1572872 | tf_op jit(solution)/shard_map/ppermute | solution.py:125
  114.0 7.9 %collective-permute-start.7 = (bf16[256,256]{1,0:T(8,128)(2,1)S(1)}, bf16[256,256]{1,0:T(8,128)(2,1)S(1)}, u32[]{:S(2)}, u32[]{:S(2)}) collective-permute-start(bf16[256,256]{1,0:T(8,128)(2,1)S(1)} %slice.216), channel_id=1, source_target_pairs={{0,16},{4,20},{8,24},{12,28},{16,0},{20,4},{24,8},{28,12},{1,17},{... | collective-permute-start | bytes 393224 | tf_op jit(solution)/shard_map/ppermute | solution.py:125
  118.1 9.4 %collective-permute-start.6 = (bf16[512,256]{1,0:T(8,128)(2,1)S(1)}, bf16[512,256]{1,0:T(8,128)(2,1)S(1)}, u32[]{:S(2)}, u32[]{:S(2)}) collective-permute-start(bf16[512,256]{1,0:T(8,128)(2,1)S(1)} %concatenate.182), channel_id=1, source_target_pairs={{0,8},{4,12},{8,0},{12,4},{16,24},{20,28},{24,16},{28,20},{1,9},{5... | collective-permute-start | bytes 786440 | tf_op jit(solution)/shard_map/ppermute | solution.py:125
  120.6 35.8 %collective-permute-start.8 = (bf16[1024,256]{1,0:T(8,128)(2,1)}, bf16[1024,256]{1,0:T(8,128)(2,1)}, u32[]{:S(2)}, u32[]{:S(2)}) collective-permute-start(bf16[1024,256]{1,0:T(8,128)(2,1)} %pad_maximum_fusion.10), channel_id=1, source_target_pairs={{0,8},{4,12},{8,0},{12,4},{16,24},{20,28},{24,16},{28,20},{1,9},{5... | collective-permute-start | bytes 1572872 | tf_op jit(solution)/shard_map/ppermute | solution.py:125
  127.5 3.7 %collective-permute-start.21 = (f32[4,512]{1,0:T(4,128)S(1)}, f32[4,512]{1,0:T(4,128)S(1)}, u32[]{:S(2)}, u32[]{:S(2)}) collective-permute-start(f32[4,512]{1,0:T(4,128)S(1)} %bitcast.38), channel_id=1, source_target_pairs={{0,4},{4,0},{8,12},{12,8},{16,20},{20,16},{24,28},{28,24},{1,5},{5... | collective-permute-start | bytes 24584 | tf_op jit(solution)/shard_map/ppermute | solution.py:125
  129.4 33.1 %collective-permute-start.12 = (bf16[1024,256]{1,0:T(8,128)(2,1)}, bf16[1024,256]{1,0:T(8,128)(2,1)}, u32[]{:S(2)}, u32[]{:S(2)}) collective-permute-start(bf16[1024,256]{1,0:T(8,128)(2,1)} %pad_maximum_fusion.12), channel_id=1, source_target_pairs={{0,8},{4,12},{8,0},{12,4},{16,24},{20,28},{24,16},{28,20},{1,9},{5... | collective-permute-start | bytes 1572872 | tf_op jit(solution)/shard_map/ppermute | solution.py:125
  131.1 16.3 %collective-permute-start.22 = (f32[4,512]{1,0:T(4,128)S(1)}, f32[4,512]{1,0:T(4,128)S(1)}, u32[]{:S(2)}, u32[]{:S(2)}) collective-permute-start(f32[4,512]{1,0:T(4,128)S(1)} %add.143), channel_id=1, source_target_pairs={{0,8},{4,12},{8,0},{12,4},{16,24},{20,28},{24,16},{28,20},{1,9},{5... | collective-permute-start | bytes 24584 | tf_op jit(solution)/shard_map/ppermute | solution.py:125
  147.4 4.7 %collective-permute-start.23 = (f32[4,512]{1,0:T(4,128)S(1)}, f32[4,512]{1,0:T(4,128)S(1)}, u32[]{:S(2)}, u32[]{:S(2)}) collective-permute-start(f32[4,512]{1,0:T(4,128)S(1)} %add.144), channel_id=1, source_target_pairs={{0,16},{4,20},{8,24},{12,28},{16,0},{20,4},{24,8},{28,12},{1,17},{... | collective-permute-start | bytes 24584 | tf_op jit(solution)/shard_map/ppermute | solution.py:125
  148.9 7.5 %collective-permute-start.10 = (bf16[256,256]{1,0:T(8,128)(2,1)S(1)}, bf16[256,256]{1,0:T(8,128)(2,1)S(1)}, u32[]{:S(2)}, u32[]{:S(2)}) collective-permute-start(bf16[256,256]{1,0:T(8,128)(2,1)S(1)} %slice.215), channel_id=1, source_target_pairs={{0,16},{4,20},{8,24},{12,28},{16,0},{20,4},{24,8},{28,12},{1,17},{... | collective-permute-start | bytes 393224 | tf_op jit(solution)/shard_map/ppermute | solution.py:125
  152.1 8.9 %collective-permute-start.14 = (bf16[512,256]{1,0:T(8,128)(2,1)S(1)}, bf16[512,256]{1,0:T(8,128)(2,1)S(1)}, u32[]{:S(2)}, u32[]{:S(2)}) collective-permute-start(bf16[512,256]{1,0:T(8,128)(2,1)S(1)} %concatenate.180), channel_id=1, source_target_pairs={{0,8},{4,12},{8,0},{12,4},{16,24},{20,28},{24,16},{28,20},{1,9},{5... | collective-permute-start | bytes 786440 | tf_op jit(solution)/shard_map/ppermute | solution.py:125
  157.9 4.5 %copy-start.4 = (f32[1024,256]{1,0:T(8,128)}, f32[1024,256]{1,0:T(8,128)S(1)}, u32[]{:S(2)}) copy-start(f32[1024,256]{1,0:T(8,128)S(1)} %maximum_add_fusion.2) | copy-start | bytes 3145732
  158.0 10.5 %collective-permute-start.11 = (bf16[512,256]{1,0:T(8,128)(2,1)S(1)}, bf16[512,256]{1,0:T(8,128)(2,1)S(1)}, u32[]{:S(2)}, u32[]{:S(2)}) collective-permute-start(bf16[512,256]{1,0:T(8,128)(2,1)S(1)} %concatenate.181), channel_id=1, source_target_pairs={{0,4},{4,0},{8,12},{12,8},{16,20},{20,16},{24,28},{28,24},{1,5},{5... | collective-permute-start | bytes 786440 | tf_op jit(solution)/shard_map/ppermute | solution.py:125
  162.5 6.0 %slice-start = ((f32[1024,256]{1,0:T(8,128)}), f32[512,256]{1,0:T(8,128)S(1)}, s32[]{:S(2)}) async-start(f32[1024,256]{1,0:T(8,128)} %copy-done.4), calls=%async_computation | async-start | bytes 1048576 | tf_op jit(solution)/shard_map/concatenate | solution.py:151
  164.1 8.6 %copy-start.6 = (f32[1024,256]{1,0:T(8,128)}, f32[1024,256]{1,0:T(8,128)S(1)}, u32[]{:S(2)}) copy-start(f32[1024,256]{1,0:T(8,128)S(1)} %maximum_add_fusion.4) | copy-start | bytes 3145732
  164.1 8.6 %slice-start.3 = ((f32[512,256]{1,0:T(8,128)}), f32[256,256]{1,0:T(8,128)S(1)}, s32[]{:S(2)}) async-start(f32[512,256]{1,0:T(8,128)} %copy-done.7), calls=%async_computation.3 | async-start | bytes 524288 | tf_op jit(solution)/shard_map/slice | solution.py:151
  164.2 13.9 %slice-start.1 = ((f32[1024,256]{1,0:T(8,128)}), f32[512,256]{1,0:T(8,128)S(1)}, s32[]{:S(2)}) async-start(f32[1024,256]{1,0:T(8,128)} %copy-done.5), calls=%async_computation.1 | async-start | bytes 1048576 | tf_op jit(solution)/shard_map/concatenate | solution.py:151
  164.2 8.5 %collective-permute-start.17 = (bf16[256,256]{1,0:T(8,128)(2,1)S(1)}, bf16[256,256]{1,0:T(8,128)(2,1)S(1)}, u32[]{:S(2)}, u32[]{:S(2)}) collective-permute-start(bf16[256,256]{1,0:T(8,128)(2,1)S(1)} %slice.214), channel_id=1, source_target_pairs={{0,16},{4,20},{8,24},{12,28},{16,0},{20,4},{24,8},{28,12},{1,17},{... | collective-permute-start | bytes 393224 | tf_op jit(solution)/shard_map/ppermute | solution.py:125
  165.3 12.8 %collective-permute-start.16 = (bf16[512,256]{1,0:T(8,128)(2,1)S(1)}, bf16[512,256]{1,0:T(8,128)(2,1)S(1)}, u32[]{:S(2)}, u32[]{:S(2)}) collective-permute-start(bf16[512,256]{1,0:T(8,128)(2,1)S(1)} %concatenate.178), channel_id=1, source_target_pairs={{0,8},{4,12},{8,0},{12,4},{16,24},{20,28},{24,16},{28,20},{1,9},{5... | collective-permute-start | bytes 786440 | tf_op jit(solution)/shard_map/ppermute | solution.py:125
  167.3 10.9 %collective-permute-start.15 = (bf16[512,256]{1,0:T(8,128)(2,1)S(1)}, bf16[512,256]{1,0:T(8,128)(2,1)S(1)}, u32[]{:S(2)}, u32[]{:S(2)}) collective-permute-start(bf16[512,256]{1,0:T(8,128)(2,1)S(1)} %concatenate.179), channel_id=1, source_target_pairs={{0,4},{4,0},{8,12},{12,8},{16,20},{20,16},{24,28},{28,24},{1,5},{5... | collective-permute-start | bytes 786440 | tf_op jit(solution)/shard_map/ppermute | solution.py:125
  168.6 10.6 %collective-permute-start.20 = (bf16[256,256]{1,0:T(8,128)(2,1)S(1)}, bf16[256,256]{1,0:T(8,128)(2,1)S(1)}, u32[]{:S(2)}, u32[]{:S(2)}) collective-permute-start(bf16[256,256]{1,0:T(8,128)(2,1)S(1)} %slice.211), channel_id=1, source_target_pairs={{0,16},{4,20},{8,24},{12,28},{16,0},{20,4},{24,8},{28,12},{1,17},{... | collective-permute-start | bytes 393224 | tf_op jit(solution)/shard_map/ppermute | solution.py:125
  179.2 10.6 %collective-permute-start.19 = (bf16[256,256]{1,0:T(8,128)(2,1)S(1)}, bf16[256,256]{1,0:T(8,128)(2,1)S(1)}, u32[]{:S(2)}, u32[]{:S(2)}) collective-permute-start(bf16[256,256]{1,0:T(8,128)(2,1)S(1)} %slice.212), channel_id=1, source_target_pairs={{0,16},{4,20},{8,24},{12,28},{16,0},{20,4},{24,8},{28,12},{1,17},{... | collective-permute-start | bytes 393224 | tf_op jit(solution)/shard_map/ppermute | solution.py:125
  179.3 12.5 %collective-permute-start.18 = (bf16[256,256]{1,0:T(8,128)(2,1)S(1)}, bf16[256,256]{1,0:T(8,128)(2,1)S(1)}, u32[]{:S(2)}, u32[]{:S(2)}) collective-permute-start(bf16[256,256]{1,0:T(8,128)(2,1)S(1)} %slice.213), channel_id=1, source_target_pairs={{0,16},{4,20},{8,24},{12,28},{16,0},{20,4},{24,8},{28,12},{1,17},{... | collective-permute-start | bytes 393224 | tf_op jit(solution)/shard_map/ppermute | solution.py:125
  182.2 11.6 %copy-start.1 = (bf16[2048,512]{1,0:T(8,128)(2,1)S(1)}, bf16[2048,512]{1,0:T(8,128)(2,1)}, u32[]{:S(2)}) copy-start(bf16[2048,512]{1,0:T(8,128)(2,1)} %param.8) | copy-start | bytes 6291460
  (24 other events, 37.3 us)
where the time goes:
time: 194 us
  waiting for transfers between devices  62.7 us (32%)
  starting transfers between devices  45.8 us (24%)
  matrix products  30 us (15%)
  Pallas kernels  27.1 us (14%)
  other arithmetic  13.5 us (7%)
  local copies, waits for them, and re-layouts  13 us (7%)
    ppermute x21, waiting for transfers between devices, swap(): return lax.ppermute(block, 'sp', [(i, i ^ 1 << bit) for i in range(size)])  49.5 us
    ppermute x21, starting transfers between devices, swap(): return lax.ppermute(block, 'sp', [(i, i ^ 1 << bit) for i in range(size)])  37.9 us
    pallas_call x2, Pallas kernels, attention(): pl.pallas_call(attention_kernel, grid=(heads,), in_specs=[pl.BlockSpec(me...  27.1 us
    dot_general x24, matrix products, product(): jnp.einsum('td,tc->dc', piece, grads, preferred_element_type=jnp.float32)  19.2 us
    ppermute x3, waiting for transfers between devices, from_behind(): return lax.ppermute(block, axis, route)  13.3 us
    dot_general x3, matrix products, project(): jnp.dot(inputs, weight, preferred_element_type=jnp.float32)  10.8 us
    ppermute x3, starting transfers between devices, from_behind(): return lax.ppermute(block, axis, route)  7.88 us
    unnamed x91, local copies, waits for them, and re-layouts  5.74 us
  transfers between devices with their start and end apart: 24, of which 15 were waited for; matrix products, arithmetic and copies ran while one was open for 17% of the time, Pallas kernels for 0%

commit v1 on v0

--- a/solution.py
+++ b/solution.py
@@ -191,7 +191,8 @@
         dv = lax.dynamic_update_slice(dv, (tv + back[:, span:]).astype(jnp.bfloat16), (rows - REACH, 0))
         for i, grad in ((1, dk), (2, dv)):
             order = orders[3 * group + i]
-            flying.append(swap(leading(pieces, grad, order), order[0]))
+            sent = leading(pieces, grad, order)
+            flying.append(swap(sent, order[0]))
         grads.append((dq, dk, dv))
         chunks.extend((dq, dk, dv))
         diags.append(diag)
@@ -199,7 +200,9 @@
     kept = [[r for p in range(low) if not p >> order[0] & 1 for r in members[p]] for order in orders]
     held = [None] * count
     steps = sorted(((c, s) for c in range(count) for s in range(bits)), key=lambda cs: (ready[cs[0]] + 0.95 * cs[1], cs))
-    last = None
+    last, done, hop = None, 0, 0
+    diag = jnp.concatenate(diags, axis=0)[:, 0, :]
+    table_came = swap(diag, 0)
     for c, stage in steps:
         came = flying[c]
         if last is not None:
@@ -213,13 +216,16 @@
             out, held[c], kept[c] = split(held[c], kept[c], bit)
             flying[c] = swap(out, bit)
         last = c
+        done += 1
+        if hop < bits and done >= len(steps) * (hop + 1) // (bits + 1):
+            came, held[c] = lax.optimization_barrier((table_came, held[c]))
+            diag = diag + came
+            hop += 1
+            if hop < bits:
+                table_came = swap(diag, hop)
     sums = [held[3 * group : 3 * group + 3] for group in range(GROUPS)]
     query_grad, key_grad, value_grad = [jnp.concatenate(parts, axis=1) for parts in zip(*grads)]
     wq, wk, wv = [jnp.concatenate(parts, axis=1) for parts in zip(*sums)]
-    diag = jnp.concatenate(diags, axis=0)[:, 0, :]
-    diag, _ = lax.optimization_barrier((diag, held[0]))
-    for bit in range(bits):
-        diag = diag + swap(diag, bit)
     top = jnp.sum(diag[:, : MAXREL + 1], axis=1, keepdims=True) + jnp.sum(diag[:, 3 * MAXREL :], axis=1, keepdims=True)
     table_grad = jnp.concatenate(
         [jnp.zeros((head_count, 1), jnp.float32), diag[:, MAXREL + 1 : 3 * MAXREL][:, ::-1], top], axis=1)
@@ -231,7 +237,7 @@
     turned = [1, 0] + plain[2:] if bits > 1 else plain
     count = 3 * GROUPS
     orders = [plain] * (count - 2) + [turned] * 2
-    ready = [1.0 + i for i in range(count - 2)] + [count - 2.1, count - 1.9]
+    ready = [1.0, 3.0, 4.0, 2.0, 3.9, 4.1]
     return orders, ready
 
 

time: 194 us -> 190 us (0.979)
  waiting for transfers between devices: 62.7 us -> 74.3 us
  starting transfers between devices: 45.8 us -> 38.6 us
  other arithmetic: 13.5 us -> 8.06 us
  matrix products: 30 us -> 24.7 us
  local copies, waits for them, and re-layouts: 13 us -> 15.5 us
    ppermute x3, waiting for transfers between devices: 13.3 us -> 26 us  [from_behind(): return lax.ppermute(block, axis, route)]
    ppermute x21, starting transfers between devices: 37.9 us -> 30.7 us  [swap(): return lax.ppermute(block, 'sp', [(i, i ^ 1 << bit) for i in range(size)])]
    dot_general x24, matrix products: 19.2 us -> 13.9 us  [product(): jnp.einsum('td,tc->dc', piece, grads, preferred_element_type=jnp.float32)]
    add x6, other arithmetic: 4.64 us -> 0.62 us  [remainder(): return total + came.astype(jnp.float32)]
    concatenate x6, other arithmetic: 2.6 us -> 0.21 us  [leading(): jnp.concatenate([p.astype(jnp.bfloat16) for p in product(side(pieces, ord...]
    unnamed x91 -> x83, local copies, waits for them, and re-layouts: 5.74 us -> 7.05 us
  transfers between devices with their start and end apart: 24 -> 24, of which waited for: 15 -> 13; matrix products, arithmetic and copies ran while one was open for 17% -> 13% of each run, Pallas kernels for 0% -> 0%
where the time goes in v1:
time: 190 us
  waiting for transfers between devices  74.3 us (39%)
  starting transfers between devices  38.6 us (20%)
  Pallas kernels  27.1 us (14%)
  matrix products  24.7 us (13%)
  local copies, waits for them, and re-layouts  15.5 us (8%)
  other arithmetic  8.06 us (4%)
    ppermute x21, waiting for transfers between devices, swap(): return lax.ppermute(block, 'sp', [(i, i ^ 1 << bit) for i in range(size)])  48.4 us
    ppermute x21, starting transfers between devices, swap(): return lax.ppermute(block, 'sp', [(i, i ^ 1 << bit) for i in range(size)])  30.7 us
    pallas_call x2, Pallas kernels, attention(): pl.pallas_call(attention_kernel, grid=(heads,), in_specs=[pl.BlockSpec(me...  27.1 us
    ppermute x3, waiting for transfers between devices, from_behind(): return lax.ppermute(block, axis, route)  26 us
    dot_general x24, matrix products, product(): jnp.einsum('td,tc->dc', piece, grads, preferred_element_type=jnp.float32)  13.9 us
    dot_general x3, matrix products, project(): jnp.dot(inputs, weight, preferred_element_type=jnp.float32)  10.8 us
    ppermute x3, starting transfers between devices, from_behind(): return lax.ppermute(block, axis, route)  7.88 us
    unnamed x83, local copies, waits for them, and re-layouts  7.05 us
  transfers between devices with their start and end apart: 24, of which 13 were waited for; matrix products, arithmetic and copies ran while one was open for 13% of the time, Pallas kernels for 0%

profile of v1, /device:TPU:0, one launch (start us, length us, event | category | flops | bytes accessed | tf_op | source)
XLA Modules:
  0.0 190.0 jit_solution(14675780066422264306)
XLA Ops:
  0.7 1.6 copy-done
  2.2 5.2 %convolution_convert_fusion.1.k_ref = bf16[1024,512]{1,0:T(8,128)(2,1)S(1)} fusion(bf16[1024,2048]{1,0:T(8,128)(2,1)} %param.6, bf16[2048,512]{1,0:T(8,128)(2,1)S(1)} %copy-done), kind=kOutput, calls=%fused_computation.1 | convolution fusion | flops 2148007936 | bytes 7340032 | tf_op jit(solution)/shard_map/dot_general | solution.py:27
  7.5 2.3 %convolution_convert_fusion.v_ref = bf16[1024,512]{1,0:T(8,128)(2,1)S(1)} fusion(bf16[1024,2048]{1,0:T(8,128)(2,1)S(1)} %copy-done.2, bf16[2048,512]{1,0:T(8,128)(2,1)S(1)} %copy-done.38), kind=kOutput, calls=%fused_computation | convolution fusion | flops 2148007936 | bytes 7340032 | tf_op jit(solution)/shard_map/dot_general | solution.py:27
  9.9 1.0 copy-done.34
  10.9 5.1 %collective-permute-start = (bf16[256,1024]{1,0:T(8,128)(2,1)S(1)}, bf16[256,1024]{1,0:T(8,128)(2,1)S(1)}, u32[]{:S(2)}, u32[]{:S(2)}) collective-permute-start(bf16[256,1024]{1,0:T(8,128)(2,1)S(1)} %pad_maximum_fusion.7), channel_id=1, source_target_pairs={{0,4},{4,8},{8,12},{12,16},{16,20},{20,24},{24,28},{1,5},{5,9},{9,... | collective-permute-start | bytes 1572872 | tf_op jit(solution)/shard_map/ppermute | solution.py:23
  17.1 3.8 %constant_dynamic-slice_fusion.3 = (bf16[1024,256]{1,0:T(8,128)(2,1)}, bf16[1024,256]{1,0:T(8,128)(2,1)}, bf16[1024,256]{1,0:T(8,128)(2,1)S(1)}, bf16[1024,256]{...) fusion(bf16[1024,2048]{1,0:T(8,128)(2,1)} %param.6, ...), kind=kLoop, calls=%fused_computation.84 | loop fusion | bytes 8388640 | tf_op jit(solution)/shard_map/dynamic_slice | solution.py:173
  21.0 1.0 copy-done.39
  22.1 3.3 %convolution_convert_fusion.2.q_ref = bf16[1024,512]{1,0:T(8,128)(2,1)} fusion(bf16[1024,2048]{1,0:T(8,128)(2,1)S(1)} %copy-done.3, bf16[2048,512]{1,0:T(8,128)(2,1)S(1)} %copy-done.39), kind=kOutput, calls=%fused_computation.2 | convolution fusion | flops 2148007936 | bytes 7340032 | tf_op jit(solution)/shard_map/dot_general | solution.py:27
  25.4 1.6 collective-permute-done
  27.0 0.8 fusion.21
  27.8 13.5 %shard_map.117 = (bf16[1024,256]{1,0:T(8,128)(2,1)}, bf16[1024,256]{1,0:T(8,128)(2,1)}, bf16[1024,256]{1,0:T(8,128)(2,1)}, bf16[256,256]{1,0:T(8,128)(2,1)}, bf1...) custom-call(s32[1]{0:T(128)} %bitcast.first_ref, ...), custom_call_target="tpu_custom_call" | custom-call | flops 2415919104 | bytes 5242880 | tf_op jit(solution)/shard_map/pallas_call | solution.py:101
  41.3 1.6 convolution_convert_fusion.14
  43.9 13.6 %shard_map.118 = (bf16[1024,256]{1,0:T(8,128)(2,1)}, bf16[1024,256]{1,0:T(8,128)(2,1)}, bf16[1024,256]{1,0:T(8,128)(2,1)}, bf16[256,256]{1,0:T(8,128)(2,1)}, bf1...) custom-call(s32[1]{0:T(128)} %bitcast.first_ref, ...), custom_call_target="tpu_custom_call" | custom-call | flops 2415919104 | bytes 5242880 | tf_op jit(solution)/shard_map/pallas_call | solution.py:101
  57.5 1.7 convolution_convert_fusion.11
  61.3 1.1 pad_maximum_fusion.2
  62.4 2.5 %collective-permute-start.3 = (bf16[1024,256]{1,0:T(8,128)(2,1)S(1)}, bf16[1024,256]{1,0:T(8,128)(2,1)S(1)}, u32[]{:S(2)}, u32[]{:S(2)}) collective-permute-start(bf16[1024,256]{1,0:T(8,128)(2,1)S(1)} %pad_maximum_fusion.9), channel_id=1, source_target_pairs={{0,4},{4,0},{8,12},{12,8},{16,20},{20,16},{24,28},{28,24},{1,5},{5... | collective-permute-start | bytes 1572872 | tf_op jit(solution)/shard_map/ppermute | solution.py:125
  65.1 2.0 %collective-permute-start.7 = (f32[4,512]{1,0:T(4,128)S(1)}, f32[4,512]{1,0:T(4,128)S(1)}, u32[]{:S(2)}, u32[]{:S(2)}) collective-permute-start(f32[4,512]{1,0:T(4,128)S(1)} %bitcast.41), channel_id=1, source_target_pairs={{0,4},{4,0},{8,12},{12,8},{16,20},{20,16},{24,28},{28,24},{1,5},{5... | collective-permute-start | bytes 24584 | tf_op jit(solution)/shard_map/ppermute | solution.py:125
  67.1 1.3 collective-permute-start.1
  68.4 1.5 collective-permute-start.2
  71.0 23.8 %collective-permute-done.1 = bf16[256,512]{1,0:T(8,128)(2,1)S(1)} collective-permute-done((bf16[256,512]{1,0:T(8,128)(2,1)S(1)}, bf16[256,512]{1,0:T(8,128)(2,1)S(1)}, u32[]{:S(2)}, u32[]{:S(2)}) %collective-permute-start.1) | collective-permute-done | bytes 262176 | tf_op jit(solution)/shard_map/ppermute | solution.py:23
  103.4 1.5 pad_maximum_fusion.3
  105.1 3.1 %collective-permute-start.9 = (bf16[1024,256]{1,0:T(8,128)(2,1)S(1)}, bf16[1024,256]{1,0:T(8,128)(2,1)S(1)}, u32[]{:S(2)}, u32[]{:S(2)}) collective-permute-start(bf16[1024,256]{1,0:T(8,128)(2,1)S(1)} %pad_maximum_fusion.10), channel_id=1, source_target_pairs={{0,8},{4,12},{8,0},{12,4},{16,24},{20,28},{24,16},{28,20},{1,9},{5... | collective-permute-start | bytes 1572872 | tf_op jit(solution)/shard_map/ppermute | solution.py:125
  110.0 13.6 %collective-permute-done.5 = bf16[512,256]{1,0:T(8,128)(2,1)S(1)} collective-permute-done((bf16[512,256]{1,0:T(8,128)(2,1)S(1)}, bf16[512,256]{1,0:T(8,128)(2,1)S(1)}, u32[]{:S(2)}, u32[]{:S(2)}) %collective-permute-start.5) | collective-permute-done | bytes 262176 | tf_op jit(solution)/shard_map/ppermute | solution.py:125
  123.6 1.7 collective-permute-start.12
  125.4 3.2 %collective-permute-start.8 = (bf16[256,256]{1,0:T(8,128)(2,1)S(1)}, bf16[256,256]{1,0:T(8,128)(2,1)S(1)}, u32[]{:S(2)}, u32[]{:S(2)}) collective-permute-start(bf16[256,256]{1,0:T(8,128)(2,1)S(1)} %slice.216), channel_id=1, source_target_pairs={{0,16},{4,20},{8,24},{12,28},{16,0},{20,4},{24,8},{28,12},{1,17},{... | collective-permute-start | bytes 393224 | tf_op jit(solution)/shard_map/ppermute | solution.py:125
  128.8 4.3 %collective-permute-done.8 = bf16[256,256]{1,0:T(8,128)(2,1)S(1)} collective-permute-done((bf16[256,256]{1,0:T(8,128)(2,1)S(1)}, bf16[256,256]{1,0:T(8,128)(2,1)S(1)}, u32[]{:S(2)}, u32[]{:S(2)}) %collective-permute-start.8) | collective-permute-done | bytes 131104 | tf_op jit(solution)/shard_map/ppermute | solution.py:125
  133.4 1.8 collective-permute-start.19
  135.2 8.4 %collective-permute-done.6 = bf16[512,256]{1,0:T(8,128)(2,1)S(1)} collective-permute-done((bf16[512,256]{1,0:T(8,128)(2,1)S(1)}, bf16[512,256]{1,0:T(8,128)(2,1)S(1)}, u32[]{:S(2)}, u32[]{:S(2)}) %collective-permute-start.6) | collective-permute-done | bytes 262176 | tf_op jit(solution)/shard_map/ppermute | solution.py:125
  143.8 3.7 %collective-permute-start.11 = (bf16[256,256]{1,0:T(8,128)(2,1)S(1)}, bf16[256,256]{1,0:T(8,128)(2,1)S(1)}, u32[]{:S(2)}, u32[]{:S(2)}) collective-permute-start(bf16[256,256]{1,0:T(8,128)(2,1)S(1)} %slice.215), channel_id=1, source_target_pairs={{0,16},{4,20},{8,24},{12,28},{16,0},{20,4},{24,8},{28,12},{1,17},{... | collective-permute-start | bytes 393224 | tf_op jit(solution)/shard_map/ppermute | solution.py:125
  147.6 5.5 %collective-permute-done.11 = bf16[256,256]{1,0:T(8,128)(2,1)S(1)} collective-permute-done((bf16[256,256]{1,0:T(8,128)(2,1)S(1)}, bf16[256,256]{1,0:T(8,128)(2,1)S(1)}, u32[]{:S(2)}, u32[]{:S(2)}) %collective-permute-start.11) | collective-permute-done | bytes 131104 | tf_op jit(solution)/shard_map/ppermute | solution.py:125
  153.1 0.8 collective-permute-start.14
  154.2 0.9 pad_maximum_fusion.12
  155.0 4.4 %collective-permute-done.14 = bf16[512,256]{1,0:T(8,128)(2,1)S(1)} collective-permute-done((bf16[512,256]{1,0:T(8,128)(2,1)S(1)}, bf16[512,256]{1,0:T(8,128)(2,1)S(1)}, u32[]{:S(2)}, u32[]{:S(2)}) %collective-permute-start.14) | collective-permute-done | bytes 262176 | tf_op jit(solution)/shard_map/ppermute | solution.py:125
  159.7 0.6 copy-done.8
  160.3 0.7 concatenate.180
  161.2 0.7 concatenate.178
  161.9 4.8 %collective-permute-start.17 = (bf16[256,256]{1,0:T(8,128)(2,1)S(1)}, bf16[256,256]{1,0:T(8,128)(2,1)S(1)}, u32[]{:S(2)}, u32[]{:S(2)}) collective-permute-start(bf16[256,256]{1,0:T(8,128)(2,1)S(1)} %slice.214), channel_id=1, source_target_pairs={{0,16},{4,20},{8,24},{12,28},{16,0},{20,4},{24,8},{28,12},{1,17},{... | collective-permute-start | bytes 393224 | tf_op jit(solution)/shard_map/ppermute | solution.py:125
  166.8 0.6 collective-permute-start.22
  167.5 0.7 slice.212
  168.2 2.8 %collective-permute-start.21 = (bf16[256,256]{1,0:T(8,128)(2,1)}, bf16[256,256]{1,0:T(8,128)(2,1)S(1)}, u32[]{:S(2)}, u32[]{:S(2)}) collective-permute-start(bf16[256,256]{1,0:T(8,128)(2,1)} %slice.212), channel_id=1, source_target_pairs={{0,16},{4,20},{8,24},{12,28},{16,0},{20,4},{24,8},{28,12},{1,17},{... | collective-permute-start | bytes 393224 | tf_op jit(solution)/shard_map/ppermute | solution.py:125
  172.4 0.7 pad_maximum_fusion.21
  173.0 4.4 %collective-permute-done.15 = bf16[512,256]{1,0:T(8,128)(2,1)} collective-permute-done((bf16[512,256]{1,0:T(8,128)(2,1)}, bf16[512,256]{1,0:T(8,128)(2,1)}, u32[]{:S(2)}, u32[]{:S(2)}) %collective-permute-start.15) | collective-permute-done | bytes 262176 | tf_op jit(solution)/shard_map/ppermute | solution.py:125
  177.5 1.0 convert_add_fusion.1
  178.7 1.2 collective-permute-start.20
  179.9 1.8 collective-permute-start.23
  181.7 4.3 %collective-permute-done.20 = bf16[256,256]{1,0:T(8,128)(2,1)S(1)} collective-permute-done((bf16[256,256]{1,0:T(8,128)(2,1)S(1)}, bf16[256,256]{1,0:T(8,128)(2,1)S(1)}, u32[]{:S(2)}, u32[]{:S(2)}) %collective-permute-start.20) | collective-permute-done | bytes 131104 | tf_op jit(solution)/shard_map/ppermute | solution.py:125
  186.0 2.8 %collective-permute-done.23 = bf16[256,256]{1,0:T(8,128)(2,1)S(1)} collective-permute-done((bf16[256,256]{1,0:T(8,128)(2,1)S(1)}, bf16[256,256]{1,0:T(8,128)(2,1)S(1)}, u32[]{:S(2)}, u32[]{:S(2)}) %collective-permute-start.23) | collective-permute-done | bytes 131104 | tf_op jit(solution)/shard_map/ppermute | solution.py:125
  188.9 1.1 pad_maximum_fusion.15
  (198 shorter events, 18.8 us)
Async XLA Ops:
  0.6 6.8 %copy-start.2 = (bf16[1024,2048]{1,0:T(8,128)(2,1)S(1)}, bf16[1024,2048]{1,0:T(8,128)(2,1)}, u32[]{:S(2)}) copy-start(bf16[1024,2048]{1,0:T(8,128)(2,1)} %param.6) | copy-start | bytes 12582916
  0.7 6.8 %copy-start.38 = (bf16[2048,512]{1,0:T(8,128)(2,1)S(1)}, bf16[2048,512]{1,0:T(8,128)(2,1)}, u32[]{:S(2)}) copy-start(bf16[2048,512]{1,0:T(8,128)(2,1)} %param.9) | copy-start | bytes 6291460
  7.5 8.5 %copy-start.35 = (f32[4,257]{1,0:T(4,128)S(1)}, f32[4,257]{1,0:T(4,128)}, u32[]{:S(2)}) copy-start(f32[4,257]{1,0:T(4,128)} %param.10) | copy-start | bytes 12340
  10.9 16.1 %collective-permute-start = (bf16[256,1024]{1,0:T(8,128)(2,1)S(1)}, bf16[256,1024]{1,0:T(8,128)(2,1)S(1)}, u32[]{:S(2)}, u32[]{:S(2)}) collective-permute-start(bf16[256,1024]{1,0:T(8,128)(2,1)S(1)} %pad_maximum_fusion.7), channel_id=1, source_target_pairs={{0,4},{4,8},{8,12},{12,16},{16,20},{20,24},{24,28},{1,5},{5,9},{9,... | collective-permute-start | bytes 1572872 | tf_op jit(solution)/shard_map/ppermute | solution.py:23
  17.1 4.9 %copy-start.39 = (bf16[2048,512]{1,0:T(8,128)(2,1)S(1)}, bf16[2048,512]{1,0:T(8,128)(2,1)}, u32[]{:S(2)}) copy-start(bf16[2048,512]{1,0:T(8,128)(2,1)} %param.7) | copy-start | bytes 6291460
  22.1 35.4 %copy-start.21 = (bf16[1024,256]{1,0:T(8,128)(2,1)}, bf16[1024,256]{1,0:T(8,128)(2,1)S(1)}, u32[]{:S(2)}) copy-start(bf16[1024,256]{1,0:T(8,128)(2,1)S(1)} %get-tuple-element.127) | copy-start | bytes 1572868
  22.1 38.7 %copy-start.18 = (bf16[1024,256]{1,0:T(8,128)(2,1)}, bf16[1024,256]{1,0:T(8,128)(2,1)S(1)}, u32[]{:S(2)}) copy-start(bf16[1024,256]{1,0:T(8,128)(2,1)S(1)} %get-tuple-element.131) | copy-start | bytes 1572868
  61.3 7.1 %copy-start.29 = (bf16[256,256]{1,0:T(8,128)(2,1)S(1)}, bf16[256,256]{1,0:T(8,128)(2,1)}, u32[]{:S(2)}) copy-start(bf16[256,256]{1,0:T(8,128)(2,1)} %get-tuple-element.76) | copy-start | bytes 393220
  61.3 7.1 %copy-start.30 = (bf16[256,256]{1,0:T(8,128)(2,1)S(1)}, bf16[256,256]{1,0:T(8,128)(2,1)}, u32[]{:S(2)}) copy-start(bf16[256,256]{1,0:T(8,128)(2,1)} %get-tuple-element.77) | copy-start | bytes 393220
  61.3 8.6 %copy-start.16 = (bf16[1024,256]{1,0:T(8,128)(2,1)S(1)}, bf16[1024,256]{1,0:T(8,128)(2,1)}, u32[]{:S(2)}) copy-start(bf16[1024,256]{1,0:T(8,128)(2,1)} %get-tuple-element.125) | copy-start | bytes 1572868
  61.3 8.6 %copy-start.17 = (bf16[1024,256]{1,0:T(8,128)(2,1)S(1)}, bf16[1024,256]{1,0:T(8,128)(2,1)}, u32[]{:S(2)}) copy-start(bf16[1024,256]{1,0:T(8,128)(2,1)} %get-tuple-element.126) | copy-start | bytes 1572868
  62.4 63.0 %collective-permute-start.3 = (bf16[1024,256]{1,0:T(8,128)(2,1)S(1)}, bf16[1024,256]{1,0:T(8,128)(2,1)S(1)}, u32[]{:S(2)}, u32[]{:S(2)}) collective-permute-start(bf16[1024,256]{1,0:T(8,128)(2,1)S(1)} %pad_maximum_fusion.9), channel_id=1, source_target_pairs={{0,4},{4,0},{8,12},{12,8},{16,20},{20,16},{24,28},{28,24},{1,5},{5... | collective-permute-start | bytes 1572872 | tf_op jit(solution)/shard_map/ppermute | solution.py:125
  65.0 44.2 %collective-permute-start.4 = (bf16[1024,256]{1,0:T(8,128)(2,1)S(1)}, bf16[1024,256]{1,0:T(8,128)(2,1)S(1)}, u32[]{:S(2)}, u32[]{:S(2)}) collective-permute-start(bf16[1024,256]{1,0:T(8,128)(2,1)S(1)} %pad_maximum_fusion.8), channel_id=1, source_target_pairs={{0,4},{4,0},{8,12},{12,8},{16,20},{20,16},{24,28},{28,24},{1,5},{5... | collective-permute-start | bytes 1572872 | tf_op jit(solution)/shard_map/ppermute | solution.py:125
  65.1 68.3 %collective-permute-start.7 = (f32[4,512]{1,0:T(4,128)S(1)}, f32[4,512]{1,0:T(4,128)S(1)}, u32[]{:S(2)}, u32[]{:S(2)}) collective-permute-start(f32[4,512]{1,0:T(4,128)S(1)} %bitcast.41), channel_id=1, source_target_pairs={{0,4},{4,0},{8,12},{12,8},{16,20},{20,16},{24,28},{28,24},{1,5},{5... | collective-permute-start | bytes 24584 | tf_op jit(solution)/shard_map/ppermute | solution.py:125
  67.1 27.7 %collective-permute-start.1 = (bf16[256,512]{1,0:T(8,128)(2,1)S(1)}, bf16[256,512]{1,0:T(8,128)(2,1)S(1)}, u32[]{:S(2)}, u32[]{:S(2)}) collective-permute-start(bf16[256,512]{1,0:T(8,128)(2,1)S(1)} %pad_maximum_fusion.17), channel_id=1, source_target_pairs={{4,0},{8,4},{12,8},{16,12},{20,16},{24,20},{28,24},{5,1},{9,5},{13... | collective-permute-start | bytes 786440 | tf_op jit(solution)/shard_map/ppermute | solution.py:23
  68.4 30.3 %collective-permute-start.2 = (bf16[256,512]{1,0:T(8,128)(2,1)S(1)}, bf16[256,512]{1,0:T(8,128)(2,1)S(1)}, u32[]{:S(2)}, u32[]{:S(2)}) collective-permute-start(bf16[256,512]{1,0:T(8,128)(2,1)S(1)} %pad_maximum_fusion.18), channel_id=1, source_target_pairs={{4,0},{8,4},{12,8},{16,12},{20,16},{24,20},{28,24},{5,1},{9,5},{13... | collective-permute-start | bytes 786440 | tf_op jit(solution)/shard_map/ppermute | solution.py:23
  70.5 24.4 %copy-start.12 = (bf16[1024,256]{1,0:T(8,128)(2,1)S(1)}, bf16[1024,256]{1,0:T(8,128)(2,1)}, u32[]{:S(2)}) copy-start(bf16[1024,256]{1,0:T(8,128)(2,1)} %get-tuple-element.71) | copy-start | bytes 1572868
  70.5 24.4 %copy-start.13 = (bf16[1024,256]{1,0:T(8,128)(2,1)S(1)}, bf16[1024,256]{1,0:T(8,128)(2,1)}, u32[]{:S(2)}) copy-start(bf16[1024,256]{1,0:T(8,128)(2,1)} %get-tuple-element.78) | copy-start | bytes 1572868
  70.5 24.4 %copy-start.25 = (f32[256,256]{1,0:T(8,128)S(1)}, f32[256,256]{1,0:T(8,128)}, u32[]{:S(2)}) copy-start(f32[256,256]{1,0:T(8,128)} %get-tuple-element.72) | copy-start | bytes 786436
  70.5 24.4 %copy-start.26 = (f32[256,256]{1,0:T(8,128)S(1)}, f32[256,256]{1,0:T(8,128)}, u32[]{:S(2)}) copy-start(f32[256,256]{1,0:T(8,128)} %get-tuple-element.79) | copy-start | bytes 786436
  105.0 38.8 %collective-permute-start.10 = (bf16[1024,256]{1,0:T(8,128)(2,1)S(1)}, bf16[1024,256]{1,0:T(8,128)(2,1)S(1)}, u32[]{:S(2)}, u32[]{:S(2)}) collective-permute-start(bf16[1024,256]{1,0:T(8,128)(2,1)S(1)} %pad_maximum_fusion.11), channel_id=1, source_target_pairs={{0,4},{4,0},{8,12},{12,8},{16,20},{20,16},{24,28},{28,24},{1,5},{5... | collective-permute-start | bytes 1572872 | tf_op jit(solution)/shard_map/ppermute | solution.py:125
  105.1 48.8 %collective-permute-start.9 = (bf16[1024,256]{1,0:T(8,128)(2,1)S(1)}, bf16[1024,256]{1,0:T(8,128)(2,1)S(1)}, u32[]{:S(2)}, u32[]{:S(2)}) collective-permute-start(bf16[1024,256]{1,0:T(8,128)(2,1)S(1)} %pad_maximum_fusion.10), channel_id=1, source_target_pairs={{0,8},{4,12},{8,0},{12,4},{16,24},{20,28},{24,16},{28,20},{1,9},{5... | collective-permute-start | bytes 1572872 | tf_op jit(solution)/shard_map/ppermute | solution.py:125
  109.3 14.2 %collective-permute-start.5 = (bf16[512,256]{1,0:T(8,128)(2,1)S(1)}, bf16[512,256]{1,0:T(8,128)(2,1)S(1)}, u32[]{:S(2)}, u32[]{:S(2)}) collective-permute-start(bf16[512,256]{1,0:T(8,128)(2,1)S(1)} %concatenate.183), channel_id=1, source_target_pairs={{0,8},{4,12},{8,0},{12,4},{16,24},{20,28},{24,16},{28,20},{1,9},{5... | collective-permute-start | bytes 786440 | tf_op jit(solution)/shard_map/ppermute | solution.py:125
  123.6 36.0 %collective-permute-start.12 = (bf16[1024,256]{1,0:T(8,128)(2,1)S(1)}, bf16[1024,256]{1,0:T(8,128)(2,1)S(1)}, u32[]{:S(2)}, u32[]{:S(2)}) collective-permute-start(bf16[1024,256]{1,0:T(8,128)(2,1)S(1)} %pad_maximum_fusion.13), channel_id=1, source_target_pairs={{0,4},{4,0},{8,12},{12,8},{16,20},{20,16},{24,28},{28,24},{1,5},{5... | collective-permute-start | bytes 1572872 | tf_op jit(solution)/shard_map/ppermute | solution.py:125
  125.4 7.6 %collective-permute-start.8 = (bf16[256,256]{1,0:T(8,128)(2,1)S(1)}, bf16[256,256]{1,0:T(8,128)(2,1)S(1)}, u32[]{:S(2)}, u32[]{:S(2)}) collective-permute-start(bf16[256,256]{1,0:T(8,128)(2,1)S(1)} %slice.216), channel_id=1, source_target_pairs={{0,16},{4,20},{8,24},{12,28},{16,0},{20,4},{24,8},{28,12},{1,17},{... | collective-permute-start | bytes 393224 | tf_op jit(solution)/shard_map/ppermute | solution.py:125
  133.1 10.6 %collective-permute-start.6 = (bf16[512,256]{1,0:T(8,128)(2,1)S(1)}, bf16[512,256]{1,0:T(8,128)(2,1)S(1)}, u32[]{:S(2)}, u32[]{:S(2)}) collective-permute-start(bf16[512,256]{1,0:T(8,128)(2,1)S(1)} %concatenate.182), channel_id=1, source_target_pairs={{0,8},{4,12},{8,0},{12,4},{16,24},{20,28},{24,16},{28,20},{1,9},{5... | collective-permute-start | bytes 786440 | tf_op jit(solution)/shard_map/ppermute | solution.py:125
  133.4 27.6 %collective-permute-start.19 = (bf16[1024,256]{1,0:T(8,128)(2,1)S(1)}, bf16[1024,256]{1,0:T(8,128)(2,1)S(1)}, u32[]{:S(2)}, u32[]{:S(2)}) collective-permute-start(bf16[1024,256]{1,0:T(8,128)(2,1)S(1)} %pad_maximum_fusion.14), channel_id=1, source_target_pairs={{0,8},{4,12},{8,0},{12,4},{16,24},{20,28},{24,16},{28,20},{1,9},{5... | collective-permute-start | bytes 1572872 | tf_op jit(solution)/shard_map/ppermute | solution.py:125
  143.6 15.9 %collective-permute-start.13 = (f32[4,512]{1,0:T(4,128)S(1)}, f32[4,512]{1,0:T(4,128)S(1)}, u32[]{:S(2)}, u32[]{:S(2)}) collective-permute-start(f32[4,512]{1,0:T(4,128)S(1)} %fusion.8), channel_id=1, source_target_pairs={{0,8},{4,12},{8,0},{12,4},{16,24},{20,28},{24,16},{28,20},{1,9},{5... | collective-permute-start | bytes 24584 | tf_op jit(solution)/shard_map/ppermute | solution.py:125
  143.8 9.3 %collective-permute-start.11 = (bf16[256,256]{1,0:T(8,128)(2,1)S(1)}, bf16[256,256]{1,0:T(8,128)(2,1)S(1)}, u32[]{:S(2)}, u32[]{:S(2)}) collective-permute-start(bf16[256,256]{1,0:T(8,128)(2,1)S(1)} %slice.215), channel_id=1, source_target_pairs={{0,16},{4,20},{8,24},{12,28},{16,0},{20,4},{24,8},{28,12},{1,17},{... | collective-permute-start | bytes 393224 | tf_op jit(solution)/shard_map/ppermute | solution.py:125
  147.6 6.5 %copy-start.6 = (f32[1024,256]{1,0:T(8,128)}, f32[1024,256]{1,0:T(8,128)S(1)}, u32[]{:S(2)}) copy-start(f32[1024,256]{1,0:T(8,128)S(1)} %maximum_add_fusion.2) | copy-start | bytes 3145732
  153.1 6.4 %collective-permute-start.14 = (bf16[512,256]{1,0:T(8,128)(2,1)S(1)}, bf16[512,256]{1,0:T(8,128)(2,1)S(1)}, u32[]{:S(2)}, u32[]{:S(2)}) collective-permute-start(bf16[512,256]{1,0:T(8,128)(2,1)S(1)} %concatenate.181), channel_id=1, source_target_pairs={{0,8},{4,12},{8,0},{12,4},{16,24},{20,28},{24,16},{28,20},{1,9},{5... | collective-permute-start | bytes 786440 | tf_op jit(solution)/shard_map/ppermute | solution.py:125
  154.0 5.5 %copy-start.5 = (f32[1024,256]{1,0:T(8,128)}, f32[1024,256]{1,0:T(8,128)S(1)}, u32[]{:S(2)}) copy-start(f32[1024,256]{1,0:T(8,128)S(1)} %maximum_add_fusion.4) | copy-start | bytes 3145732
  154.1 5.4 %slice-start.2 = ((f32[1024,256]{1,0:T(8,128)}), f32[512,256]{1,0:T(8,128)S(1)}, s32[]{:S(2)}) async-start(f32[1024,256]{1,0:T(8,128)} %copy-done.6), calls=%async_computation.2 | async-start | bytes 1048576 | tf_op jit(solution)/shard_map/concatenate | solution.py:151
  154.1 13.3 %collective-permute-start.18 = (bf16[512,256]{1,0:T(8,128)(2,1)S(1)}, bf16[512,256]{1,0:T(8,128)(2,1)S(1)}, u32[]{:S(2)}, u32[]{:S(2)}) collective-permute-start(bf16[512,256]{1,0:T(8,128)(2,1)S(1)} %concatenate.179), channel_id=1, source_target_pairs={{0,4},{4,0},{8,12},{12,8},{16,20},{20,16},{24,28},{28,24},{1,5},{5... | collective-permute-start | bytes 786440 | tf_op jit(solution)/shard_map/ppermute | solution.py:125
  161.1 6.4 %slice-start.1 = ((f32[1024,256]{1,0:T(8,128)}), f32[512,256]{1,0:T(8,128)S(1)}, s32[]{:S(2)}) async-start(f32[1024,256]{1,0:T(8,128)} %copy-done.5), calls=%async_computation.1 | async-start | bytes 1048576 | tf_op jit(solution)/shard_map/concatenate | solution.py:151
  161.2 10.4 %copy-start.7 = (f32[1024,256]{1,0:T(8,128)}, f32[1024,256]{1,0:T(8,128)S(1)}, u32[]{:S(2)}) copy-start(f32[1024,256]{1,0:T(8,128)S(1)} %maximum_add_fusion.5) | copy-start | bytes 3145732
  161.2 10.3 %slice-start.4 = ((f32[512,256]{1,0:T(8,128)}), f32[256,256]{1,0:T(8,128)S(1)}, s32[]{:S(2)}) async-start(f32[512,256]{1,0:T(8,128)} %copy-done.8), calls=%async_computation.4 | async-start | bytes 524288 | tf_op jit(solution)/shard_map/slice | solution.py:151
  161.2 16.3 %slice-start = ((f32[1024,256]{1,0:T(8,128)}), f32[512,256]{1,0:T(8,128)S(1)}, s32[]{:S(2)}) async-start(f32[1024,256]{1,0:T(8,128)} %copy-done.4), calls=%async_computation | async-start | bytes 1048576 | tf_op jit(solution)/shard_map/concatenate | solution.py:151
  161.9 9.6 %collective-permute-start.17 = (bf16[256,256]{1,0:T(8,128)(2,1)S(1)}, bf16[256,256]{1,0:T(8,128)(2,1)S(1)}, u32[]{:S(2)}, u32[]{:S(2)}) collective-permute-start(bf16[256,256]{1,0:T(8,128)(2,1)S(1)} %slice.214), channel_id=1, source_target_pairs={{0,16},{4,20},{8,24},{12,28},{16,0},{20,4},{24,8},{28,12},{1,17},{... | collective-permute-start | bytes 393224 | tf_op jit(solution)/shard_map/ppermute | solution.py:125
  166.7 5.0 %collective-permute-start.16 = (f32[4,512]{1,0:T(4,128)S(1)}, f32[4,512]{1,0:T(4,128)S(1)}, u32[]{:S(2)}, u32[]{:S(2)}) collective-permute-start(f32[4,512]{1,0:T(4,128)S(1)} %add.136), channel_id=1, source_target_pairs={{0,16},{4,20},{8,24},{12,28},{16,0},{20,4},{24,8},{28,12},{1,17},{... | collective-permute-start | bytes 24584 | tf_op jit(solution)/shard_map/ppermute | solution.py:125
  166.8 10.7 %collective-permute-start.15 = (bf16[512,256]{1,0:T(8,128)(2,1)}, bf16[512,256]{1,0:T(8,128)(2,1)}, u32[]{:S(2)}, u32[]{:S(2)}) collective-permute-start(bf16[512,256]{1,0:T(8,128)(2,1)} %concatenate.180), channel_id=1, source_target_pairs={{0,8},{4,12},{8,0},{12,4},{16,24},{20,28},{24,16},{28,20},{1,9},{5... | collective-permute-start | bytes 786440 | tf_op jit(solution)/shard_map/ppermute | solution.py:125
  166.8 11.7 %collective-permute-start.22 = (bf16[512,256]{1,0:T(8,128)(2,1)}, bf16[512,256]{1,0:T(8,128)(2,1)S(1)}, u32[]{:S(2)}, u32[]{:S(2)}) collective-permute-start(bf16[512,256]{1,0:T(8,128)(2,1)} %concatenate.178), channel_id=1, source_target_pairs={{0,4},{4,0},{8,12},{12,8},{16,20},{20,16},{24,28},{28,24},{1,5},{5... | collective-permute-start | bytes 786440 | tf_op jit(solution)/shard_map/ppermute | solution.py:125
  168.2 10.4 %collective-permute-start.21 = (bf16[256,256]{1,0:T(8,128)(2,1)}, bf16[256,256]{1,0:T(8,128)(2,1)S(1)}, u32[]{:S(2)}, u32[]{:S(2)}) collective-permute-start(bf16[256,256]{1,0:T(8,128)(2,1)} %slice.212), channel_id=1, source_target_pairs={{0,16},{4,20},{8,24},{12,28},{16,0},{20,4},{24,8},{28,12},{1,17},{... | collective-permute-start | bytes 393224 | tf_op jit(solution)/shard_map/ppermute | solution.py:125
  171.7 6.8 %slice-start.3 = ((f32[1024,256]{1,0:T(8,128)}), f32[512,256]{1,0:T(8,128)S(1)}, s32[]{:S(2)}) async-start(f32[1024,256]{1,0:T(8,128)} %copy-done.7), calls=%async_computation.3 | async-start | bytes 1048576 | tf_op jit(solution)/shard_map/concatenate | solution.py:151
  173.0 8.6 %slice-start.5 = ((f32[512,256]{1,0:T(8,128)}), f32[256,256]{1,0:T(8,128)S(1)}, s32[]{:S(2)}) async-start(f32[512,256]{1,0:T(8,128)} %copy-done.9), calls=%async_computation.5 | async-start | bytes 524288 | tf_op jit(solution)/shard_map/slice | solution.py:151
  178.6 11.3 %copy-start.1 = (bf16[2048,512]{1,0:T(8,128)(2,1)S(1)}, bf16[2048,512]{1,0:T(8,128)(2,1)}, u32[]{:S(2)}) copy-start(bf16[2048,512]{1,0:T(8,128)(2,1)} %param.8) | copy-start | bytes 6291460
  178.7 7.3 %collective-permute-start.20 = (bf16[256,256]{1,0:T(8,128)(2,1)S(1)}, bf16[256,256]{1,0:T(8,128)(2,1)S(1)}, u32[]{:S(2)}, u32[]{:S(2)}) collective-permute-start(bf16[256,256]{1,0:T(8,128)(2,1)S(1)} %slice.213), channel_id=1, source_target_pairs={{0,16},{4,20},{8,24},{12,28},{16,0},{20,4},{24,8},{28,12},{1,17},{... | collective-permute-start | bytes 393224 | tf_op jit(solution)/shard_map/ppermute | solution.py:125
  179.9 8.9 %collective-permute-start.23 = (bf16[256,256]{1,0:T(8,128)(2,1)S(1)}, bf16[256,256]{1,0:T(8,128)(2,1)S(1)}, u32[]{:S(2)}, u32[]{:S(2)}) collective-permute-start(bf16[256,256]{1,0:T(8,128)(2,1)S(1)} %slice.211), channel_id=1, source_target_pairs={{0,16},{4,20},{8,24},{12,28},{16,0},{20,4},{24,8},{28,12},{1,17},{... | collective-permute-start | bytes 393224 | tf_op jit(solution)/shard_map/ppermute | solution.py:125
  (22 other events, 38.9 us)
